TPU v7x, 32 devices: a whole 2x2x4 slice. The times are simulated.
32 devices in a mesh: grp: 2 (over x), tp: 4 (over z), dp: 4 (over y, core).
Axes of the slice: x: 2, y: 2, z: 4, core: 2. Of those that a mesh axis runs over, the one named last changes fastest.
Arguments:
- stream: bfloat16 [32, 4096], P('grp', 'dp'), parts along dimension 0, may hold values from -11 to 11
- states: float32 [2, 32, 32, 64, 64], P(None, ('grp', 'dp'), 'tp'), parts along dimension 1, may hold values from -6 to 6
- norm_gain: bfloat16 [2, 4096], P(None, 'dp'), may hold values from 0.099609375 to 1.8984375
- recept_weight: bfloat16 [2, 4096, 2048], P(None, 'dp', 'tp'), may hold values from -0.09375 to 0.09375
- key_weight: bfloat16 [2, 4096, 2048], P(None, 'dp', 'tp'), may hold values from -0.09375 to 0.09375
- value_weight: bfloat16 [2, 4096, 2048], P(None, 'dp', 'tp'), may hold values from -0.09375 to 0.09375
- decay_weight: bfloat16 [2, 4096, 2048], P(None, 'dp', 'tp'), may hold values from -0.09375 to 0.09375
- rate_weight: bfloat16 [2, 4096, 2048], P(None, 'dp', 'tp'), may hold values from -0.09375 to 0.09375
- gate_weight: bfloat16 [2, 4096, 2048], P(None, 'dp', 'tp'), may hold values from -0.09375 to 0.09375
- out_weight: bfloat16 [2, 2048, 4096], P(None, 'tp', 'dp'), may hold values from -0.125 to 0.125
- decay_bias: float32 [2, 2048], P(None, 'tp'), may hold values from -2 to 2
- head_gain: bfloat16 [2, 2048], P(None, 'tp'), may hold values from 0.099609375 to 1.8984375
Outputs:
- new_stream: bfloat16 [32, 4096], P('grp', 'dp'), parts along dimension 0
- new_states: float32 [2, 32, 32, 64, 64], P(None, ('grp', 'dp'), 'tp'), parts along dimension 1
There are 2 independent parts, one for each index of `grp`. A program takes and returns all parts, laid end to end along the dimension named above; an argument that names none is the same for every part. Nothing has to cross between parts.
All inputs are finite; a program needn't handle non-finite values.
Results may differ from a plain program's by a relative error of at most 0.0068.
Values may be sent and summed in bfloat16 or wider, within the bound.
A program may use at most 64 MiB of HBM per device.

v0:
```python
import jax
import jax.numpy as jnp
from jax import lax
from jax.sharding import PartitionSpec as P

D = 4096
HEAD = 64


def run_block(stream, state_blk, gain, weights, out_weight, bias, hgain):
    current = stream.astype(jnp.float32)
    squares = jnp.sum(current * current, axis=1)
    normed = (current * gain.astype(jnp.float32)).astype(jnp.bfloat16)
    width = weights[0].shape[1]
    local_rows = state_blk.shape[0]
    all_totals = lax.psum(squares, "dp")
    offset = lax.axis_index("dp") * local_rows
    totals = lax.dynamic_slice_in_dim(all_totals, offset, local_rows, 0)
    summed = lax.psum_scatter(
        jnp.concatenate(
            [jnp.dot(normed, weight, preferred_element_type=jnp.float32) for weight in weights],
            axis=1,
        ),
        "dp",
        scatter_dimension=0,
        tiled=True,
    )
    inv_rms = lax.rsqrt(totals / D + 1e-06)[:, None]
    projected = (summed * inv_rms).reshape(local_rows, 6, -1, HEAD)
    recept = projected[:, 0]
    key_vec = projected[:, 1]
    value_vec = projected[:, 2]
    decay_pre = projected[:, 3]
    rate_pre = projected[:, 4]
    gate_pre = projected[:, 5]
    unit_key = key_vec * lax.rsqrt(jnp.sum(key_vec * key_vec, axis=2, keepdims=True) + 1e-06)
    rate_vec = jax.nn.sigmoid(rate_pre)
    decay = jnp.exp(-0.606531 * jax.nn.sigmoid(bias.reshape(1, -1, HEAD) + decay_pre))
    removed = jnp.einsum("bhij,bhj->bhi", state_blk, unit_key, precision=lax.Precision.HIGHEST)
    new_state = (
        state_blk * decay[:, :, None, :]
        - removed[..., None] * (unit_key * rate_vec)[:, :, None, :]
        + value_vec[..., None] * key_vec[:, :, None, :]
    )
    read = jnp.einsum("bhij,bhj->bhi", new_state, recept, precision=lax.Precision.HIGHEST)
    center = read - jnp.mean(read, axis=2, keepdims=True)
    normal_read = center * lax.rsqrt(jnp.mean(center * center, axis=2, keepdims=True) + 1e-05)
    gated = normal_read * hgain.astype(jnp.float32).reshape(1, -1, HEAD) * jax.nn.sigmoid(gate_pre)
    mixed = gated.reshape(local_rows, width).astype(jnp.bfloat16)
    branch_part = jnp.dot(
        lax.all_gather(mixed, "dp", axis=0, tiled=True),
        out_weight,
        preferred_element_type=jnp.float32,
    )
    branch = lax.psum(branch_part, "tp")
    return ((current + branch).astype(jnp.bfloat16), new_state)


def per_device(
    stream,
    states,
    norm_gain,
    recept_weight,
    key_weight,
    value_weight,
    decay_weight,
    rate_weight,
    gate_weight,
    out_weight,
    decay_bias,
    head_gain,
):
    current = stream
    fresh_list = []
    for layer in range(2):
        weights = (
            recept_weight[layer],
            key_weight[layer],
            value_weight[layer],
            decay_weight[layer],
            rate_weight[layer],
            gate_weight[layer],
        )
        current, fresh = run_block(
            current,
            states[layer],
            norm_gain[layer],
            weights,
            out_weight[layer],
            decay_bias[layer],
            head_gain[layer],
        )
        fresh_list.append(fresh)
    return (current, jnp.stack(fresh_list))


def solution(mesh):
    in_specs = (
        P("grp", "dp"),
        P(None, ("grp", "dp"), "tp", None, None),
        P(None, "dp"),
        P(None, "dp", "tp"),
        P(None, "dp", "tp"),
        P(None, "dp", "tp"),
        P(None, "dp", "tp"),
        P(None, "dp", "tp"),
        P(None, "dp", "tp"),
        P(None, "tp", "dp"),
        P(None, "tp"),
        P(None, "tp"),
    )
    out_specs = (P("grp", "dp"), P(None, ("grp", "dp"), "tp", None, None))
    return jax.shard_map(
        per_device, mesh=mesh, in_specs=in_specs, out_specs=out_specs, check_vma=False
    )
```

profile of v0, /device:TPU:0, one launch (start us, length us, event | category | flops | bytes accessed | tf_op | source)
XLA Modules:
  0.0 201.3 jit_solution(15151777179491624203)
XLA Ops:
  8.1 1.6 convolution_dynamic-update-slice_fusion.11
  9.7 1.5 convolution_dynamic-update-slice_fusion.10
  11.5 1.6 convolution_dynamic-update-slice_fusion.8
  13.4 1.5 convolution_dynamic-update-slice_fusion.6
  15.8 8.4 %psum.28 = f32[16]{0:T(128)S(1)} all-reduce(f32[16]{0:T(128)S(1)} %fusion.61), channel_id=1, replica_groups=mesh['grp'=2,'tp'=4,'dp'=4] {'dp'}, use_global_device_ids=true, to_apply=%region_2.0 | all-reduce | flops 16 | bytes 128 | tf_op jit(solution)/shard_map/psum | solution.py:16
  25.7 24.8 %all-reduce.11.cloned.1.call-done = f32[16,3072]{1,0:T(8,128)} async-done(((f32[16,3072]{1,0:T(8,128)}), f32[16,3072]{1,0:T(8,128)}) %all-reduce.11.cloned.1.call-update) | async-done | bytes 196624
  51.7 1.7 fusion.22
  53.5 2.1 %fusion.26 = f32[4,8,1,64]{3,2,1,0:T(1,128)S(1)} fusion(f32[4,8,64,1]{2,3,1,0:T(1,128)S(1)} %bitcast.192, f32[2,4,8,64,64]{4,3,2,1,0:T(8,128)S(1)} %copy-done, f32[4,8,64]{2,1,0:T(8,128)S(1)} %get-tuple-element.23, f32[4,8,64]{2,1,0:T(8,128)S(1)} %get-tuple-element.21, f32[4,8,64]{2,1,0:T(8,128)S(1)} %get-tuple-element.10, f32[4,8,64]{2,1,0:T(8,128)S(1)} %bitcast.185, ...), kind=kOutput, calls=%fused_computation.40 | convolution fusion | flops 2228224 | bytes 1155072 | tf_op jit(solution)/shard_map/bhij,bhj->bhi/dot_general | solution.py:45
  56.0 5.2 %all-gather = bf16[4,4,512]{2,1,0:T(4,128)(2,1)S(1)} all-gather(bf16[1,4,512]{2,1,0:T(4,128)(2,1)S(1)} %reshape.168), channel_id=1, replica_groups=mesh['grp'=2,'tp'=4,'dp'=4] {'dp'}, dimensions={0}, use_global_device_ids=true | all-gather | bytes 20480 | tf_op jit(solution)/shard_map/all_gather | solution.py:51
  61.2 2.1 %fusion.14 = f32[16,1024]{1,0:T(8,128)} fusion(bf16[16,512]{1,0:T(8,128)(2,1)S(1)} %reshape.169, bf16[2,512,1024]{2,1,0:T(8,128)(2,1)} %param.21), kind=kOutput, calls=%fused_computation.27 | convolution fusion | flops 16777216 | bytes 1130496 | tf_op jit(solution)/shard_map/dot_general | solution.py:50
  63.5 34.3 %all-reduce.7.cloned.1.call-done = f32[16,1024]{1,0:T(8,128)} async-done(((f32[16,1024]{1,0:T(8,128)}), f32[16,1024]{1,0:T(8,128)}) %all-reduce.7.cloned.1.call-update) | async-done | bytes 65552 | tf_op jit(solution)/shard_map/psum | solution.py:55
  98.8 5.7 %psum.30 = f32[16]{0:T(128)S(1)} all-reduce(f32[16]{0:T(128)S(1)} %get-tuple-element.8), channel_id=1, replica_groups=mesh['grp'=2,'tp'=4,'dp'=4] {'dp'}, use_global_device_ids=true, to_apply=%region_9.0 | all-reduce | flops 16 | bytes 128 | tf_op jit(solution)/shard_map/psum | solution.py:16
  104.4 1.6 convolution_dynamic-update-slice_fusion.5
  106.1 1.5 convolution_dynamic-update-slice_fusion.4
  107.8 1.5 convolution_dynamic-update-slice_fusion.2
  109.5 1.5 convolution_dynamic-update-slice_fusion
  111.8 32.0 %all-reduce.13.cloned.1.call-done = f32[16,3072]{1,0:T(8,128)} async-done(((f32[16,3072]{1,0:T(8,128)}), f32[16,3072]{1,0:T(8,128)}) %all-reduce.13.cloned.1.call-update) | async-done | bytes 196624
  145.1 1.7 fusion.8
  146.8 2.2 %multiply_add_fusion.1 = (f32[1,4,8,64,64]{4,3,2,1,0:T(8,128)S(1)}, f32[1,4,8,64,64]{4,3,2,1,0:T(8,128)}) fusion(f32[2,4,8,64,64]{4,3,2,1,0:T(8,128)S(1)} %copy-done, f32[4,8,64]{2,1,0:T(8,128)S(1)} %get-tuple-element.23, f32[4,8,64]{2,1,0:T(8,128)S(1)} %get-tuple-element.21, f32[4,8,64]{2,1,0:T(8,128)S(1)} %get-tuple-element.10, ...), kind=kLoop, calls=%fused_computation.42 | loop fusion | flops 1310720 | bytes 2179072 | tf_op jit(solution)/shard_map/add | solution.py:41
  149.0 2.1 %fusion.12 = f32[4,8,1,64]{3,2,1,0:T(1,128)S(1)} fusion(f32[4,8,64,1]{2,3,1,0:T(1,128)S(1)} %bitcast.191, f32[2,4,8,64,64]{4,3,2,1,0:T(8,128)S(1)} %copy-done, f32[4,8,64]{2,1,0:T(8,128)S(1)} %get-tuple-element.18, f32[4,8,64]{2,1,0:T(8,128)S(1)} %get-tuple-element.16, f32[4,8,64]{2,1,0:T(8,128)S(1)} %get-tuple-element.6, f32[4,8,64]{2,1,0:T(8,128)S(1)} %bitcast.188, ...), kind=kOutput, calls=%fused_computation.26 | convolution fusion | flops 2228224 | bytes 1155072 | tf_op jit(solution)/shard_map/bhij,bhj->bhi/dot_general | solution.py:45
  151.5 5.2 %all-gather.1 = bf16[4,4,512]{2,1,0:T(4,128)(2,1)S(1)} all-gather(bf16[1,4,512]{2,1,0:T(4,128)(2,1)S(1)} %reshape.170), channel_id=1, replica_groups=mesh['grp'=2,'tp'=4,'dp'=4] {'dp'}, dimensions={0}, use_global_device_ids=true | all-gather | bytes 20480 | tf_op jit(solution)/shard_map/all_gather | solution.py:51
  156.8 2.1 %fusion = f32[16,1024]{1,0:T(8,128)} fusion(bf16[16,512]{1,0:T(8,128)(2,1)S(1)} %reshape.171, bf16[2,512,1024]{2,1,0:T(8,128)(2,1)} %param.21), kind=kOutput, calls=%fused_computation.13 | convolution fusion | flops 16777216 | bytes 1130496 | tf_op jit(solution)/shard_map/dot_general | solution.py:50
  158.9 2.8 %pad_maximum_fusion = f32[2,4,8,64,64]{4,3,2,1,0:T(8,128)} fusion(f32[1,4,8,64,64]{4,3,2,1,0:T(8,128)} %get-tuple-element.13, f32[1,4,8,64,64]{4,3,2,1,0:T(8,128)S(1)} %get-tuple-element.12), kind=kLoop, calls=%fused_computation | loop fusion | flops 262144 | bytes 2097152 | tf_op jit(solution)/shard_map/stack | solution.py:94
  161.6 31.7 %all-reduce.9.cloned.1.call-done = f32[16,1024]{1,0:T(8,128)} async-done(((f32[16,1024]{1,0:T(8,128)}), f32[16,1024]{1,0:T(8,128)}) %all-reduce.9.cloned.1.call-update) | async-done | bytes 65552 | tf_op jit(solution)/shard_map/psum | solution.py:55
  (72 shorter events, 10.5 us)
Async XLA Ops:
  7.2 4.1 %copy-start.1 = (bf16[16,1024]{1,0:T(8,128)(2,1)S(1)}, bf16[16,1024]{1,0:T(8,128)(2,1)}, u32[]{:S(2)}) copy-start(bf16[16,1024]{1,0:T(8,128)(2,1)} %param.12) | copy-start | bytes 98308
  7.2 4.1 %copy-start.2 = (bf16[2,1024,512]{2,1,0:T(8,128)(2,1)S(1)}, bf16[2,1024,512]{2,1,0:T(8,128)(2,1)}, u32[]{:S(2)}) copy-start(bf16[2,1024,512]{2,1,0:T(8,128)(2,1)} %param.17) | copy-start | bytes 6291460
  7.2 43.3 %all-reduce.11.cloned.1.call-start = ((), (), s32[]{:S(2)}) async-start(), calls=%async_computation.2 | async-start | bytes 393216
  8.1 5.0 %copy-start.4 = (bf16[2,1024,512]{2,1,0:T(8,128)(2,1)S(1)}, bf16[2,1024,512]{2,1,0:T(8,128)(2,1)}, u32[]{:S(2)}) copy-start(bf16[2,1024,512]{2,1,0:T(8,128)(2,1)} %param.19) | copy-start | bytes 6291460
  11.2 12.9 %copy-start.8 = (bf16[2,512]{1,0:T(2,128)(2,1)S(1)}, bf16[2,512]{1,0:T(2,128)(2,1)}, u32[]{:S(2)}) copy-start(bf16[2,512]{1,0:T(2,128)(2,1)} %param.23) | copy-start | bytes 6148
  11.2 12.9 %copy-start.9 = (f32[2,512]{1,0:T(2,128)S(1)}, f32[2,512]{1,0:T(2,128)}, u32[]{:S(2)}) copy-start(f32[2,512]{1,0:T(2,128)} %param.22) | copy-start | bytes 12292
  11.5 12.9 %copy-start.10 = (u32[32]{0:T(128)S(1)}, u32[32]{0:T(128)}, u32[]{:S(2)}) copy-start(u32[32]{0:T(128)} %constant.34) | copy-start | bytes 388
  11.5 40.2 %copy-start = (f32[2,4,8,64,64]{4,3,2,1,0:T(8,128)S(1)}, f32[2,4,8,64,64]{4,3,2,1,0:T(8,128)}, u32[]{:S(2)}) copy-start(f32[2,4,8,64,64]{4,3,2,1,0:T(8,128)} %param.13) | copy-start | bytes 3145732
  14.9 0.7 copy-start.6
  15.6 82.2 %all-reduce.7.cloned.1.call-start = ((), (), s32[]{:S(2)}) async-start(), calls=%async_computation | async-start | bytes 131072 | tf_op jit(solution)/shard_map/psum | solution.py:55
  63.3 80.5 %all-reduce.13.cloned.1.call-start = ((), (), s32[]{:S(2)}) async-start(), calls=%async_computation.3 | async-start | bytes 393216
  104.4 3.1 %copy-start.3 = (bf16[2,1024,512]{2,1,0:T(8,128)(2,1)S(1)}, bf16[2,1024,512]{2,1,0:T(8,128)(2,1)}, u32[]{:S(2)}) copy-start(bf16[2,1024,512]{2,1,0:T(8,128)(2,1)} %param.17) | copy-start | bytes 6291460
  104.4 4.8 %copy-start.5 = (bf16[2,1024,512]{2,1,0:T(8,128)(2,1)S(1)}, bf16[2,1024,512]{2,1,0:T(8,128)(2,1)}, u32[]{:S(2)}) copy-start(bf16[2,1024,512]{2,1,0:T(8,128)(2,1)} %param.19) | copy-start | bytes 6291460
  111.0 0.7 copy-start.7
  111.7 81.6 %all-reduce.9.cloned.1.call-start = ((), (), s32[]{:S(2)}) async-start(), calls=%async_computation.1 | async-start | bytes 131072 | tf_op jit(solution)/shard_map/psum | solution.py:55
Sparse Core Ops, SparseCore 0:
  15.7 34.7 all-reduce.10
  63.5 34.3 all-reduce.6
  111.8 31.9 all-reduce.12
  159.0 34.2 all-reduce.8
where the time goes:
time: 202 us; the launch traced here: 201 us
  waiting for transfers between devices  123 us (61%)
  matrix products  25.1 us (12%)
  blocking collectives  24.5 us (12%)
  between operations  14.5 us (7%)
  other arithmetic  11.5 us (6%)
  local copies, waits for them, and re-layouts  2.74 us (1%)
    psum x2, waiting for transfers between devices, run_block(): branch = lax.psum(branch_part, 'tp')  66 us
    unnamed x6, waiting for transfers between devices  56.8 us
    psum x2, blocking collectives, run_block(): all_totals = lax.psum(squares, 'dp')  14.1 us
    dot_general x12, matrix products, run_block(): jnp.dot(normed, weight, preferred_element_type=jnp.float32)  13.3 us
    all_gather x2, blocking collectives, run_block(): lax.all_gather(mixed, 'dp', axis=0, tiled=True)  10.4 us
    dot_general x2, matrix products, run_block(): jnp.dot(lax.all_gather(mixed, 'dp', axis=0, tiled=True), out_weight, pref...  4.2 us
    dot_general x2, matrix products, run_block(): jnp.einsum('bhij,bhj->bhi', new_state, recept, precision=lax.Precision.HI...  4.16 us
  transfers between devices with their start and end apart: 4, of which 4 were waited for; matrix products, arithmetic and copies ran while one was open for 2% of the time, Pallas kernels for 0%

commit v1 on v0

--- a/solution.py
+++ b/solution.py
@@ -52,7 +52,12 @@
         out_weight,
         preferred_element_type=jnp.float32,
     )
-    branch = lax.psum(branch_part, "tp")
+
+    def _feed_sheet(local_block):
+        r_now = lax.all_gather(local_block, axis_name="tp")
+        return jnp.sum(r_now, 0)
+
+    branch = _feed_sheet(branch_part)
     return ((current + branch).astype(jnp.bfloat16), new_state)
 
 

time: 202 us -> 161 us (0.80)
  waiting for transfers between devices: 123 us -> 57.3 us
  blocking collectives: 24.5 us -> 52.7 us
  other arithmetic: 11.5 us -> 8.65 us
    psum x2 -> x0, waiting for transfers between devices: 66 us -> none  [run_block(): branch = lax.psum(branch_part, 'tp')]
    all_gather x0 -> x2, blocking collectives: none -> 28 us  [_feed_sheet(): r_now = lax.all_gather(local_block, axis_name='tp')]
    unnamed x6 -> x4, waiting for transfers between devices: 56.8 us -> 57.3 us
  transfers between devices with their start and end apart: 4 -> 2, of which waited for: 4 -> 2; matrix products, arithmetic and copies ran while one was open for 2% -> 1% of each run, Pallas kernels for 0% -> 0%
where the time goes in v1:
time: 161 us; the launch traced here: 160 us
  waiting for transfers between devices  57.3 us (36%)
  blocking collectives  52.7 us (33%)
  matrix products  23.9 us (15%)
  between operations  14.8 us (9%)
  other arithmetic  8.65 us (5%)
  local copies, waits for them, and re-layouts  2.75 us (2%)
    unnamed x4, waiting for transfers between devices  57.3 us
    all_gather x2, blocking collectives, _feed_sheet(): r_now = lax.all_gather(local_block, axis_name='tp')  28 us
    psum x2, blocking collectives, run_block(): all_totals = lax.psum(squares, 'dp')  14.3 us
    dot_general x12, matrix products, run_block(): jnp.dot(normed, weight, preferred_element_type=jnp.float32)  13.3 us
    all_gather x2, blocking collectives, run_block(): lax.all_gather(mixed, 'dp', axis=0, tiled=True)  10.4 us
    dot_general x2, matrix products, run_block(): jnp.einsum('bhij,bhj->bhi', new_state, recept, precision=lax.Precision.HI...  4.17 us
    dot_general x2, matrix products, run_block(): jnp.einsum('bhij,bhj->bhi', state_blk, unit_key, precision=lax.Precision....  3.49 us
  transfers between devices with their start and end apart: 2, of which 2 were waited for; matrix products, arithmetic and copies ran while one was open for 1% of the time, Pallas kernels for 0%

profile of v1, /device:TPU:0, one launch (start us, length us, event | category | flops | bytes accessed | tf_op | source)
XLA Modules:
  0.0 160.1 jit_solution(5820744580700640734)
XLA Ops:
  8.1 1.6 %convolution_dynamic-update-slice_fusion.11 = f32[16,3072]{1,0:T(8,128)S(1)} fusion(bf16[2,1024,512]{2,1,0:T(8,128)(2,1)} %param.15, bf16[16,1024]{1,0:T(8,128)(2,1)} %param.12, f32[1024]{0:T(1024)S(1)} %bitcast.177), kind=kOutput, calls=%fused_computation.12 | convolution fusion | flops 16826368 | bytes 1118208 | tf_op jit(solution)/shard_map/dot_general | solution.py:21
  9.7 1.5 convolution_dynamic-update-slice_fusion.10
  11.5 1.6 %convolution_dynamic-update-slice_fusion.8 = f32[16,3072]{1,0:T(8,128)S(1)} fusion(f32[16,3072]{1,0:T(8,128)S(1)} %convolution_dynamic-update-slice_fusion.9, bf16[2,1024,512]{2,1,0:T(8,128)(2,1)} %param.18, bf16[16,1024]{1,0:T(8,128)(2,1)S(1)} %copy-done.2, f32[1024]{0:T(1024)S(1)} %bitcast.180), kind=kOutput, calls=%fused_computation.9 | convolution fusion | flops 16826368 | bytes 1118208 | tf_op jit(solution)/shard_map/dot_general | solution.py:21
  13.4 1.5 convolution_dynamic-update-slice_fusion.6
  15.8 8.4 %psum.14 = f32[16]{0:T(128)S(1)} all-reduce(f32[16]{0:T(128)S(1)} %fusion.61), channel_id=1, replica_groups=mesh['grp'=2,'tp'=4,'dp'=4] {'dp'}, use_global_device_ids=true, to_apply=%region_2.0 | all-reduce | flops 16 | bytes 128 | tf_op jit(solution)/shard_map/psum | solution.py:16
  25.8 24.6 %all-reduce.5.cloned.1.call-done = f32[16,3072]{1,0:T(8,128)} async-done(((f32[16,3072]{1,0:T(8,128)}), f32[16,3072]{1,0:T(8,128)}) %all-reduce.5.cloned.1.call-update) | async-done | bytes 196624
  51.7 1.7 %fusion.22 = f32[4,8,1,64]{3,2,1,0:T(1,128)S(1)} fusion(f32[4,8,64,1]{2,3,1,0:T(1,128)S(1)} %bitcast.193, f32[2,4,8,64,64]{4,3,2,1,0:T(8,128)S(1)} %copy-done), kind=kOutput, calls=%fused_computation.35 | convolution fusion | flops 1572864 | bytes 1073152 | tf_op jit(solution)/shard_map/bhij,bhj->bhi/dot_general | solution.py:39
  53.5 2.1 %fusion.26 = f32[4,8,1,64]{3,2,1,0:T(1,128)S(1)} fusion(f32[4,8,64,1]{2,3,1,0:T(1,128)S(1)} %bitcast.196, f32[2,4,8,64,64]{4,3,2,1,0:T(8,128)S(1)} %copy-done, f32[4,8,64]{2,1,0:T(8,128)S(1)} %get-tuple-element.23, f32[4,8,64]{2,1,0:T(8,128)S(1)} %get-tuple-element.21, f32[4,8,64]{2,1,0:T(8,128)S(1)} %get-tuple-element.10, f32[4,8,64]{2,1,0:T(8,128)S(1)} %bitcast.189, ...), kind=kOutput, calls=%fused_computation.40 | convolution fusion | flops 2228224 | bytes 1155072 | tf_op jit(solution)/shard_map/bhij,bhj->bhi/dot_general | solution.py:45
  56.0 5.2 %all-gather.2 = bf16[4,4,512]{2,1,0:T(4,128)(2,1)S(1)} all-gather(bf16[1,4,512]{2,1,0:T(4,128)(2,1)S(1)} %reshape.170), channel_id=1, replica_groups=mesh['grp'=2,'tp'=4,'dp'=4] {'dp'}, dimensions={0}, use_global_device_ids=true | all-gather | bytes 20480 | tf_op jit(solution)/shard_map/all_gather | solution.py:51
  61.2 1.5 fusion.14
  62.7 14.0 %all-gather = f32[64,1024]{1,0:T(8,128)S(1)} all-gather(f32[16,1024]{1,0:T(8,128)S(1)} %fusion.14), channel_id=2, replica_groups=mesh['grp'=2,'tp'=4,'dp'=4] {'tp'}, dimensions={0}, use_global_device_ids=true | all-gather | bytes 327680 | tf_op jit(solution)/shard_map/all_gather | solution.py:57
  76.8 5.9 %psum.15 = f32[16]{0:T(128)S(1)} all-reduce(f32[16]{0:T(128)S(1)} %get-tuple-element.8), channel_id=1, replica_groups=mesh['grp'=2,'tp'=4,'dp'=4] {'dp'}, use_global_device_ids=true, to_apply=%region_9.0 | all-reduce | flops 16 | bytes 128 | tf_op jit(solution)/shard_map/psum | solution.py:16
  82.7 1.6 %convolution_dynamic-update-slice_fusion.5 = f32[16,3072]{1,0:T(8,128)S(1)} fusion(bf16[2,1024,512]{2,1,0:T(8,128)(2,1)} %param.15, bf16[16,1024]{1,0:T(8,128)(2,1)S(1)} %get-tuple-element.9, f32[1024]{0:T(1024)S(1)} %bitcast.171), kind=kOutput, calls=%fused_computation.6 | convolution fusion | flops 16826368 | bytes 1118208 | tf_op jit(solution)/shard_map/dot_general | solution.py:21
  84.3 1.5 convolution_dynamic-update-slice_fusion.4
  86.1 1.5 convolution_dynamic-update-slice_fusion.2
  87.8 1.5 convolution_dynamic-update-slice_fusion
  90.1 32.6 %all-reduce.7.cloned.1.call-done = f32[16,3072]{1,0:T(8,128)} async-done(((f32[16,3072]{1,0:T(8,128)}), f32[16,3072]{1,0:T(8,128)}) %all-reduce.7.cloned.1.call-update) | async-done | bytes 196624
  124.0 1.7 %fusion.8 = f32[4,8,1,64]{3,2,1,0:T(1,128)S(1)} fusion(f32[4,8,64,1]{2,3,1,0:T(1,128)S(1)} %bitcast.194, f32[2,4,8,64,64]{4,3,2,1,0:T(8,128)S(1)} %copy-done), kind=kOutput, calls=%fused_computation.21 | convolution fusion | flops 1572864 | bytes 1073152 | tf_op jit(solution)/shard_map/bhij,bhj->bhi/dot_general | solution.py:39
  125.7 2.2 %multiply_add_fusion.1 = (f32[1,4,8,64,64]{4,3,2,1,0:T(8,128)S(1)}, f32[1,4,8,64,64]{4,3,2,1,0:T(8,128)}) fusion(f32[2,4,8,64,64]{4,3,2,1,0:T(8,128)S(1)} %copy-done, f32[4,8,64]{2,1,0:T(8,128)S(1)} %get-tuple-element.23, f32[4,8,64]{2,1,0:T(8,128)S(1)} %get-tuple-element.21, f32[4,8,64]{2,1,0:T(8,128)S(1)} %get-tuple-element.10, ...), kind=kLoop, calls=%fused_computation.42 | loop fusion | flops 1310720 | bytes 2179072 | tf_op jit(solution)/shard_map/add | solution.py:41
  127.9 2.1 %fusion.12 = f32[4,8,1,64]{3,2,1,0:T(1,128)S(1)} fusion(f32[4,8,64,1]{2,3,1,0:T(1,128)S(1)} %bitcast.195, f32[2,4,8,64,64]{4,3,2,1,0:T(8,128)S(1)} %copy-done, f32[4,8,64]{2,1,0:T(8,128)S(1)} %get-tuple-element.18, f32[4,8,64]{2,1,0:T(8,128)S(1)} %get-tuple-element.16, f32[4,8,64]{2,1,0:T(8,128)S(1)} %get-tuple-element.6, f32[4,8,64]{2,1,0:T(8,128)S(1)} %bitcast.192, ...), kind=kOutput, calls=%fused_computation.26 | convolution fusion | flops 2228224 | bytes 1155072 | tf_op jit(solution)/shard_map/bhij,bhj->bhi/dot_general | solution.py:45
  130.4 5.2 %all-gather.3 = bf16[4,4,512]{2,1,0:T(4,128)(2,1)S(1)} all-gather(bf16[1,4,512]{2,1,0:T(4,128)(2,1)S(1)} %reshape.172), channel_id=1, replica_groups=mesh['grp'=2,'tp'=4,'dp'=4] {'dp'}, dimensions={0}, use_global_device_ids=true | all-gather | bytes 20480 | tf_op jit(solution)/shard_map/all_gather | solution.py:51
  135.6 1.5 fusion
  137.1 14.0 %all-gather.1 = f32[64,1024]{1,0:T(8,128)S(1)} all-gather(f32[16,1024]{1,0:T(8,128)S(1)} %fusion), channel_id=3, replica_groups=mesh['grp'=2,'tp'=4,'dp'=4] {'tp'}, dimensions={0}, use_global_device_ids=true | all-gather | bytes 327680 | tf_op jit(solution)/shard_map/all_gather | solution.py:57
  151.8 1.5 pad_maximum_fusion
  (72 shorter events, 8.8 us)
Async XLA Ops:
  7.2 4.1 %copy-start.2 = (bf16[16,1024]{1,0:T(8,128)(2,1)S(1)}, bf16[16,1024]{1,0:T(8,128)(2,1)}, u32[]{:S(2)}) copy-start(bf16[16,1024]{1,0:T(8,128)(2,1)} %param.12) | copy-start | bytes 98308
  7.2 4.1 %copy-start.3 = (bf16[2,1024,512]{2,1,0:T(8,128)(2,1)S(1)}, bf16[2,1024,512]{2,1,0:T(8,128)(2,1)}, u32[]{:S(2)}) copy-start(bf16[2,1024,512]{2,1,0:T(8,128)(2,1)} %param.17) | copy-start | bytes 6291460
  7.2 43.3 %all-reduce.5.cloned.1.call-start = ((), (), s32[]{:S(2)}) async-start(), calls=%async_computation | async-start | bytes 393216
  8.1 5.0 %copy-start.5 = (bf16[2,1024,512]{2,1,0:T(8,128)(2,1)S(1)}, bf16[2,1024,512]{2,1,0:T(8,128)(2,1)}, u32[]{:S(2)}) copy-start(bf16[2,1024,512]{2,1,0:T(8,128)(2,1)} %param.19) | copy-start | bytes 6291460
  11.2 12.9 %copy-start.9 = (bf16[2,512]{1,0:T(2,128)(2,1)S(1)}, bf16[2,512]{1,0:T(2,128)(2,1)}, u32[]{:S(2)}) copy-start(bf16[2,512]{1,0:T(2,128)(2,1)} %param.23) | copy-start | bytes 6148
  11.2 12.9 %copy-start.10 = (f32[2,512]{1,0:T(2,128)S(1)}, f32[2,512]{1,0:T(2,128)}, u32[]{:S(2)}) copy-start(f32[2,512]{1,0:T(2,128)} %param.22) | copy-start | bytes 12292
  11.5 13.0 %copy-start.11 = (u32[32]{0:T(128)S(1)}, u32[32]{0:T(128)}, u32[]{:S(2)}) copy-start(u32[32]{0:T(128)} %constant.34) | copy-start | bytes 388
  11.5 40.2 %copy-start = (f32[2,4,8,64,64]{4,3,2,1,0:T(8,128)S(1)}, f32[2,4,8,64,64]{4,3,2,1,0:T(8,128)}, u32[]{:S(2)}) copy-start(f32[2,4,8,64,64]{4,3,2,1,0:T(8,128)} %param.13) | copy-start | bytes 3145732
  14.9 0.7 copy-start.7
  15.6 107.1 %all-reduce.7.cloned.1.call-start = ((), (), s32[]{:S(2)}) async-start(), calls=%async_computation.1 | async-start | bytes 393216
  82.7 3.1 %copy-start.4 = (bf16[2,1024,512]{2,1,0:T(8,128)(2,1)S(1)}, bf16[2,1024,512]{2,1,0:T(8,128)(2,1)}, u32[]{:S(2)}) copy-start(bf16[2,1024,512]{2,1,0:T(8,128)(2,1)} %param.17) | copy-start | bytes 6291460
  82.7 4.8 %copy-start.6 = (bf16[2,1024,512]{2,1,0:T(8,128)(2,1)S(1)}, bf16[2,1024,512]{2,1,0:T(8,128)(2,1)}, u32[]{:S(2)}) copy-start(bf16[2,1024,512]{2,1,0:T(8,128)(2,1)} %param.19) | copy-start | bytes 6291460
  89.3 0.7 copy-start.8
  130.0 21.8 %copy-start.1 = (f32[1,4,8,64,64]{4,3,2,1,0:T(8,128)S(1)}, f32[1,4,8,64,64]{4,3,2,1,0:T(8,128)}, u32[]{:S(2)}) copy-start(f32[1,4,8,64,64]{4,3,2,1,0:T(8,128)} %get-tuple-element.13) | copy-start | bytes 1572868
Sparse Core Ops, SparseCore 0:
  15.7 34.7 all-reduce.4
  90.1 32.5 all-reduce.6
